TPU v7x, 32 devices: a whole 2x2x4 slice. The times are simulated.
32 devices in a mesh: grp: 2 (over x), ep: 8 (over z, y), tp: 2 (over core).
Axes of the slice: x: 2, y: 2, z: 4, core: 2. Of those that a mesh axis runs over, the one named last changes fastest.
Arguments:
- tokens: bfloat16 [4096, 2048], P(('grp', 'ep', 'tp')), parts along dimension 0, may hold values from -6 to 6
- expert_ids: int32 [4096, 4], P(('grp', 'ep', 'tp')), parts along dimension 0, may hold values from 0 to 15, all different within a row; in each aligned block of 128 rows (0 to 127, 128 to 255, ...) at most 64 rows name the same one
- route_weights: float32 [4096, 4], P(('grp', 'ep', 'tp')), parts along dimension 0, may hold values from 0.05 to 1
- norm_gain: float32 [2048], replicated, may hold values from 0.1 to 1.9
- w_gate: bfloat16 [16, 2048, 896], P(('ep', 'tp')), may hold values from -0.5 to 0.5
- w_up: bfloat16 [16, 2048, 896], P(('ep', 'tp')), may hold values from -0.5 to 0.5
- w_down: bfloat16 [16, 896, 2048], P(('ep', 'tp')), may hold values from -0.0234375 to 0.0234375
Outputs:
- mixed: bfloat16 [4096, 2048], P(('grp', 'ep', 'tp')), parts along dimension 0
There are 2 independent parts, one for each index of `grp`. A program takes and returns all parts, laid end to end along the dimension named above; an argument that names none is the same for every part. Nothing has to cross between parts.
Inputs may be any that keep to these rules, and one draw needn't show every extreme that they name: `expert_ids`: each token names 4 different experts. Among the 128 tokens of one device (aligned blocks of rows) no expert is named more than 64 times, a bound that some block reaches.
All inputs are finite; a program needn't handle non-finite values.
Results may differ from a plain program's by a relative error of at most 0.0071.
Values may be sent and summed in bfloat16 or wider, within the bound.
No kernel may reach another device: no remote copies, remote signals or barrier semaphores. Data moves between devices by JAX's collectives and lax.ppermute only.
A program may use at most 64 MiB of HBM per device.

v0:
```python
import functools

import jax
import jax.numpy as jnp
from jax import lax
from jax.experimental import pallas as pl
from jax.experimental.pallas import tpu as pltpu
from jax.sharding import PartitionSpec as P


norm_eps = 1e-05
clamp_limit = 7.0
sig_alpha = 1.702


def layer_norm(tokens, norm_gain):
    values = tokens.astype(jnp.float32)
    row_mean = jnp.mean(values, -1, keepdims=True)
    centred = values - row_mean
    row_var = jnp.mean(centred * centred, -1, keepdims=True)
    scaled = centred * lax.rsqrt(row_var + norm_eps) * norm_gain
    return scaled.astype(jnp.bfloat16)


def expert_apply(inputs, gate_mat, up_mat, down_mat):
    gate_pre = jnp.dot(inputs, gate_mat, preferred_element_type=jnp.float32)
    up_pre = jnp.dot(inputs, up_mat, preferred_element_type=jnp.float32)
    gated = jnp.minimum(gate_pre, clamp_limit)
    upper = jnp.clip(up_pre, -clamp_limit, clamp_limit)
    hidden = (gated * jax.nn.sigmoid(sig_alpha * gated) * (upper + 1.0)).astype(jnp.bfloat16)
    return jnp.dot(hidden, down_mat, preferred_element_type=jnp.float32).astype(jnp.bfloat16)


def local(tokens, expert_ids, route_weights, norm_gain, w_gate, w_up, w_down):
    ep_count = lax.axis_size("ep")
    tp_count = lax.axis_size("tp")
    experts = ep_count * tp_count
    tok_rows, feat_width = tokens.shape
    top_count = expert_ids.shape[1]
    capacity = 2 * tok_rows * top_count // experts
    normed = layer_norm(tokens, norm_gain)
    flat_ids = expert_ids.reshape(-1)
    one_hot = (flat_ids[:, None] == jnp.arange(experts, dtype=jnp.int32)[None, :]).astype(jnp.int32)
    slot_index = jnp.sum((jnp.cumsum(one_hot, 0) - one_hot) * one_hot, 1)
    target = flat_ids * capacity + slot_index
    pair_token = jnp.arange(tok_rows * top_count, dtype=jnp.int32) // top_count
    buffer = (
        jnp.zeros((experts * capacity, feat_width), jnp.bfloat16).at[target].set(normed[pair_token])
    )
    buffer = buffer.reshape(experts, capacity, feat_width)
    gate_mat = w_gate[0]
    up_mat = w_up[0]
    down_mat = w_down[0]
    arrived = lax.all_to_all(buffer, ("ep", "tp"), split_axis=0, concat_axis=0, tiled=True)
    flat_rows = arrived.reshape(-1, feat_width)
    returned = lax.all_to_all(
        expert_apply(flat_rows, gate_mat, up_mat, down_mat).reshape(arrived.shape),
        ("ep", "tp"),
        split_axis=0,
        concat_axis=0,
        tiled=True,
    )
    picked = returned.reshape(experts * capacity, feat_width)[target].reshape(
        tok_rows, top_count, feat_width
    )
    combined = jnp.zeros((tok_rows, feat_width), jnp.float32)
    for choice_slot in range(top_count):
        combined = combined + route_weights[:, choice_slot : choice_slot + 1] * picked[
            :, choice_slot
        ].astype(jnp.float32)
    return combined.astype(jnp.bfloat16)


def expert_kernel(tok_rows, capacity, experts, pieces, pairs, *refs):
    number = pairs * 2 * pieces
    which = refs[0]
    blocks = refs[1 : 1 + number]
    gate_hbm, up_hbm, down_hbm, own_out, other_out = refs[1 + number : 6 + number]
    gate_mat, up_mat, down_mat, chosen, hidden, weight, spread, gather, sems = refs[6 + number :]
    feat_width, hid_width = gate_mat.shape
    tile = 256
    hid_tiles, out_tiles = hid_width // tile, feat_width // tile
    tail = hid_width - hid_tiles * tile

    def hid_copy(i, at, width):
        cols = pl.ds(at, width)
        return (
            pltpu.make_async_copy(gate_hbm.at[0, :, cols], gate_mat.at[:, cols], sems.at[0, i]),
            pltpu.make_async_copy(up_hbm.at[0, :, cols], up_mat.at[:, cols], sems.at[1, i]),
        )

    def out_copy(i, at):
        cols = pl.ds(at, tile)
        return pltpu.make_async_copy(down_hbm.at[0, :, cols], down_mat.at[:, cols], sems.at[2, i])

    for i in range(hid_tiles):
        for copy in hid_copy(i, i * tile, tile):
            copy.start()
    if tail:
        for copy in hid_copy(hid_tiles, hid_tiles * tile, tail):
            copy.start()
    for i in range(out_tiles):
        out_copy(i, i * tile).start()

    tokens, slots = 2 * tok_rows, 2 * capacity
    row = lax.broadcasted_iota(jnp.int32, (tokens, tokens), 0)
    col = lax.broadcasted_iota(jnp.int32, (tokens, tokens), 1)
    earlier = (col < row) & ((col >= tok_rows) == (row >= tok_rows))
    earlier = jnp.where(earlier, 1.0, 0.0).astype(jnp.bfloat16)
    for p in range(pairs):
        mine = blocks[p * 2 * pieces : (p + 1) * 2 * pieces]
        extra = jnp.concatenate([r[:, feat_width:] for r in mine], 0).astype(jnp.float32)
        lane = lax.broadcasted_iota(jnp.int32, extra.shape, 1)
        wanted = (lane == which[0]) | (lane == which[0] + experts)
        scale = jnp.sum(jnp.where(wanted, extra, 0.0), 1, keepdims=True)
        mask = jnp.broadcast_to(jnp.where(scale > 0.0, 1.0, 0.0), (tokens, slots))
        place = jnp.dot(earlier, mask.astype(jnp.bfloat16), preferred_element_type=jnp.float32)
        line = lax.broadcasted_iota(jnp.int32, (tokens, slots), 0)
        slot = lax.broadcasted_iota(jnp.int32, (tokens, slots), 1)
        target = place.astype(jnp.int32) + jnp.where(line >= tok_rows, capacity, 0)
        one_hot = jnp.where((target == slot) & (mask > 0.0), 1.0, 0.0)
        spread[p] = one_hot.astype(jnp.bfloat16)
        gather[p] = one_hot.T.astype(jnp.bfloat16)
        weight[p] = jnp.broadcast_to(scale, (tokens, tile))

        @pl.loop(0, feat_width // tile)
        def _(i):
            cols = pl.ds(pl.multiple_of(i * tile, tile), tile)
            part = jnp.concatenate([r[:, cols] for r in mine], 0)
            picked = jnp.dot(gather[p], part, preferred_element_type=jnp.float32)
            chosen[p * slots : (p + 1) * slots, cols] = picked.astype(jnp.bfloat16)

    def hid_tile(i, at, width):
        for copy in hid_copy(i, at, width):
            copy.wait()
        cols = pl.ds(at, width)
        gate_pre = jnp.dot(chosen[...], gate_mat[:, cols], preferred_element_type=jnp.float32)
        up_pre = jnp.dot(chosen[...], up_mat[:, cols], preferred_element_type=jnp.float32)
        gated = jnp.minimum(gate_pre, clamp_limit)
        upper = jnp.clip(up_pre, -clamp_limit, clamp_limit)
        value = gated * jax.nn.sigmoid(sig_alpha * gated) * (upper + 1.0)
        hidden[:, cols] = value.astype(jnp.bfloat16)

    @pl.loop(0, hid_tiles)
    def _(i):
        hid_tile(i, pl.multiple_of(i * tile, tile), tile)

    if tail:
        hid_tile(hid_tiles, hid_tiles * tile, tail)

    @pl.loop(0, out_tiles)
    def _(i):
        at = pl.multiple_of(i * tile, tile)
        out_copy(i, at).wait()
        cols = pl.ds(at, tile)
        out = jnp.dot(hidden[...], down_mat[:, cols], preferred_element_type=jnp.float32)
        out = out.astype(jnp.bfloat16)
        for p in range(pairs):
            full = jnp.dot(
                spread[p], out[p * slots : (p + 1) * slots], preferred_element_type=jnp.float32
            )
            full = (full * weight[p]).astype(jnp.bfloat16)
            own_out[p * tok_rows : (p + 1) * tok_rows, cols] = full[:tok_rows]
            other_out[p * tok_rows : (p + 1) * tok_rows, cols] = full[tok_rows:]


def expert_blocks(which, groups, w_gate, w_up, w_down, tok_rows, capacity, experts):
    pairs, pieces = len(groups), len(groups[0]) // 2
    flat = [v for g in groups for v in g]
    feat_width, hid_width = w_gate.shape[1:]
    tokens, slots = 2 * tok_rows, 2 * capacity
    rows = pairs * slots
    shape = jax.ShapeDtypeStruct((pairs * tok_rows, feat_width), jnp.bfloat16)
    vmem = pl.BlockSpec(memory_space=pltpu.VMEM)
    return pl.pallas_call(
        functools.partial(expert_kernel, tok_rows, capacity, experts, pieces, pairs),
        out_shape=(shape, shape),
        in_specs=[pl.BlockSpec(memory_space=pltpu.SMEM)]
        + [vmem] * len(flat)
        + [pl.BlockSpec(memory_space=pltpu.HBM)] * 3,
        out_specs=(vmem, vmem),
        scratch_shapes=[
            pltpu.VMEM((feat_width, hid_width), jnp.bfloat16),
            pltpu.VMEM((feat_width, hid_width), jnp.bfloat16),
            pltpu.VMEM((hid_width, feat_width), jnp.bfloat16),
            pltpu.VMEM((rows, feat_width), jnp.bfloat16),
            pltpu.VMEM((rows, hid_width), jnp.bfloat16),
            pltpu.VMEM((pairs, tokens, 256), jnp.float32),
            pltpu.VMEM((pairs, tokens, slots), jnp.bfloat16),
            pltpu.VMEM((pairs, slots, tokens), jnp.bfloat16),
            pltpu.SemaphoreType.DMA((3, 8)),
        ],
        compiler_params=pltpu.CompilerParams(vmem_limit_bytes=40 * 2**20),
        cost_estimate=pl.CostEstimate(
            flops=6 * rows * feat_width * hid_width,
            bytes_accessed=6 * feat_width * hid_width,
            transcendentals=rows * hid_width,
        ),
    )(which, *flat, w_gate, w_up, w_down)


def add_kernel(*refs):
    total = refs[0][...].astype(jnp.float32)
    for ref in refs[1:-1]:
        total = total + ref[...].astype(jnp.float32)
    refs[-1][...] = total.astype(jnp.bfloat16)


def add_piece(own, returned, piece, rows, arrived):
    width = own.shape[1]
    picked = pl.BlockSpec((rows, width), lambda g: (piece, 0))
    whole = pl.BlockSpec((rows, width), lambda g: (0, 0))
    return pl.pallas_call(
        add_kernel,
        grid=(1,),
        out_shape=jax.ShapeDtypeStruct((rows, width), jnp.bfloat16),
        in_specs=[picked, picked] + [whole] * len(arrived),
        out_specs=whole,
        compiler_params=pltpu.CompilerParams(vmem_limit_bytes=8 * 2**20),
        cost_estimate=pl.CostEstimate(flops=rows * width, bytes_accessed=0, transcendentals=0),
    )(own, returned, *arrived)


def ring_local(tokens, expert_ids, route_weights, norm_gain, w_gate, w_up, w_down):
    ep_count = lax.axis_size("ep")
    tp_count = lax.axis_size("tp")
    experts = ep_count * tp_count
    tok_rows, _ = tokens.shape
    capacity = 2 * tok_rows * expert_ids.shape[1] // experts
    half = ep_count // 2
    order = list(range(0, ep_count, 2)) + list(range(ep_count - 1, 0, -2))
    ahead = [(order[i], order[(i + 1) % ep_count]) for i in range(ep_count)]
    behind = [(b, a) for a, b in ahead]
    swap = [(0, 1), (1, 0)]
    pieces = 2
    rows = tok_rows // pieces
    normed = layer_norm(tokens, norm_gain)
    fits = expert_ids[:, :, None] == jnp.arange(experts, dtype=jnp.int32)
    weights = jnp.sum(jnp.where(fits, route_weights[:, :, None], 0.0), 1)
    high = weights.astype(jnp.bfloat16)
    low = (weights - high.astype(jnp.float32)).astype(jnp.bfloat16)
    lanes = -(-2 * experts // 128) * 128
    gap = jnp.zeros((tok_rows, lanes - 2 * experts), jnp.bfloat16)
    packed = jnp.concatenate([normed, high, low, gap], 1)
    start = [packed[c * rows : (c + 1) * rows] for c in range(pieces)]
    which = (lax.axis_index("ep") * tp_count + lax.axis_index("tp")).astype(jnp.int32).reshape(1)

    def shift(value, pairs):
        return lax.ppermute(value, "ep", pairs)

    def other(value):
        return lax.ppermute(value, "tp", swap)

    held = [[{} for _ in range(half + 1)] for _ in range(2)]
    for direction in range(2):
        held[direction][0] = {c: start[c] for c in range(pieces)}
    for step in range(1, half + 1):
        for c in range(pieces):
            for direction, pairs in ((0, ahead), (1, behind)):
                if step == half and c % 2 != direction:
                    continue
                held[direction][step][c] = shift(held[direction][step - 1][c], pairs)

    sums = [[{} for _ in range(half + 1)] for _ in range(2)]
    for step in range(half + 1):
        if step == 0:
            groups = [[(0, c) for c in range(pieces)]]
        elif step == half:
            groups = [[(c % 2, c) for c in range(pieces)]]
        else:
            groups = [[(d, c) for c in range(pieces)] for d in range(2)]
        values = []
        for g in groups:
            mine = [held[d][step][c] for d, c in g]
            swapped = []
            for (d, c), v in zip(g, mine):
                swapped.append(other(v))
            values.append(mine + swapped)
        own, theirs = expert_blocks(
            which, values, w_gate, w_up, w_down, tok_rows, capacity, experts
        )
        returned = other(theirs)
        for i, (d, c) in enumerate([k for g in groups for k in g]):
            sums[d][step][c] = (own, returned, i, rows)

    arrived = [{}, {}]
    for step in range(half, 0, -1):
        for direction, pairs in ((0, behind), (1, ahead)):
            for c in sorted(sums[direction][step]):
                before = [arrived[direction][c]] if c in arrived[direction] else []
                total = add_piece(*sums[direction][step][c], before)
                arrived[direction][c] = shift(total, pairs)
    done = [
        add_piece(*sums[0][0][c], [arrived[0][c], arrived[1][c]]) for c in range(pieces)
    ]
    return jnp.concatenate(done, 0)


def is_ring(mesh, tok_rows, top_count):
    ep_count, tp_count = mesh.shape["ep"], mesh.shape["tp"]
    capacity = 2 * tok_rows * top_count // (ep_count * tp_count)
    return 2 * capacity >= tok_rows and ep_count % 2 == 0 and ep_count >= 6 and tp_count == 2


def solution(mesh):
    placed = (
        P(("grp", "ep", "tp"), None),
        P(("grp", "ep", "tp"), None),
        P(("grp", "ep", "tp"), None),
        P(),
        P(("ep", "tp"), None, None),
        P(("ep", "tp"), None, None),
        P(("ep", "tp"), None, None),
    )

    def body(tokens, expert_ids, *rest):
        ring = is_ring(mesh, tokens.shape[0], expert_ids.shape[1])
        return (ring_local if ring else local)(tokens, expert_ids, *rest)

    return jax.shard_map(
        body, mesh=mesh, in_specs=placed, out_specs=P(("grp", "ep", "tp"), None), check_vma=False
    )
```

profile of v0, /device:TPU:0, one launch (start us, length us, event | category | flops | bytes accessed | tf_op | source)
XLA Modules:
  0.0 173.9 jit_solution(5257654878487913305)
XLA Ops:
  5.4 3.1 %collective-permute-start.3 = (bf16[64,2176]{1,0:T(8,128)(2,1)S(1)}, bf16[64,2176]{1,0:T(8,128)(2,1)S(1)}, u32[]{:S(2)}, u32[]{:S(2)}) collective-permute-start(bf16[64,2176]{1,0:T(8,128)(2,1)S(1)} %get-tuple-element.26.refs_1_), channel_id=1, source_target_pairs={{0,4},{4,8},{8,12},{12,14},{14,10},{10,6},{6,2},{2,0},{1,5},{5,9},... | collective-permute-start | bytes 835592 | tf_op jit(solution)/shard_map/ppermute | solution.py:249
  10.5 5.4 %collective-permute-done.3.refs_1_ = bf16[64,2176]{1,0:T(8,128)(2,1)S(1)} collective-permute-done((bf16[64,2176]{1,0:T(8,128)(2,1)S(1)}, bf16[64,2176]{1,0:T(8,128)(2,1)S(1)}, u32[]{:S(2)}, u32[]{:S(2)}) %collective-permute-start.3) | collective-permute-done | bytes 278560 | tf_op jit(solution)/shard_map/ppermute | solution.py:249
  15.9 2.1 %collective-permute-start.12 = (bf16[64,2176]{1,0:T(8,128)(2,1)S(1)}, bf16[64,2176]{1,0:T(8,128)(2,1)S(1)}, u32[]{:S(2)}, u32[]{:S(2)}) collective-permute-start(bf16[64,2176]{1,0:T(8,128)(2,1)S(1)} %collective-permute-done.3.refs_1_), channel_id=1, source_target_pairs={{0,4},{4,8},{8,12},{12,14},{14,10},{10,6},{6,2},{2,0},{1,5},{5,9},... | collective-permute-start | bytes 835592 | tf_op jit(solution)/shard_map/ppermute | solution.py:249
  18.0 3.9 %collective-permute-done.4.refs_2_ = bf16[64,2176]{1,0:T(8,128)(2,1)S(1)} collective-permute-done((bf16[64,2176]{1,0:T(8,128)(2,1)S(1)}, bf16[64,2176]{1,0:T(8,128)(2,1)S(1)}, u32[]{:S(2)}, u32[]{:S(2)}) %collective-permute-start.4) | collective-permute-done | bytes 278560 | tf_op jit(solution)/shard_map/ppermute | solution.py:249
  21.9 2.1 %collective-permute-start.13 = (bf16[64,2176]{1,0:T(8,128)(2,1)S(1)}, bf16[64,2176]{1,0:T(8,128)(2,1)S(1)}, u32[]{:S(2)}, u32[]{:S(2)}) collective-permute-start(bf16[64,2176]{1,0:T(8,128)(2,1)S(1)} %collective-permute-done.4.refs_2_), channel_id=1, source_target_pairs={{0,4},{4,8},{8,12},{12,14},{14,10},{10,6},{6,2},{2,0},{1,5},{5,9},... | collective-permute-start | bytes 835592 | tf_op jit(solution)/shard_map/ppermute | solution.py:249
  27.9 2.1 %collective-permute-start.21 = (bf16[64,2176]{1,0:T(8,128)(2,1)S(1)}, bf16[64,2176]{1,0:T(8,128)(2,1)S(1)}, u32[]{:S(2)}, u32[]{:S(2)}) collective-permute-start(bf16[64,2176]{1,0:T(8,128)(2,1)S(1)} %collective-permute-done.12.refs_1_), channel_id=1, source_target_pairs={{0,4},{4,8},{8,12},{12,14},{14,10},{10,6},{6,2},{2,0},{1,5},{5,9},... | collective-permute-start | bytes 835592 | tf_op jit(solution)/shard_map/ppermute | solution.py:249
  29.9 3.9 %collective-permute-done.13.refs_2_ = bf16[64,2176]{1,0:T(8,128)(2,1)S(1)} collective-permute-done((bf16[64,2176]{1,0:T(8,128)(2,1)S(1)}, bf16[64,2176]{1,0:T(8,128)(2,1)S(1)}, u32[]{:S(2)}, u32[]{:S(2)}) %collective-permute-start.13) | collective-permute-done | bytes 278560 | tf_op jit(solution)/shard_map/ppermute | solution.py:249
  33.8 2.1 %collective-permute-start.22 = (bf16[64,2176]{1,0:T(8,128)(2,1)S(1)}, bf16[64,2176]{1,0:T(8,128)(2,1)S(1)}, u32[]{:S(2)}, u32[]{:S(2)}) collective-permute-start(bf16[64,2176]{1,0:T(8,128)(2,1)S(1)} %collective-permute-done.13.refs_2_), channel_id=1, source_target_pairs={{0,4},{4,8},{8,12},{12,14},{14,10},{10,6},{6,2},{2,0},{1,5},{5,9},... | collective-permute-start | bytes 835592 | tf_op jit(solution)/shard_map/ppermute | solution.py:249
  39.8 5.1 %collective-permute-done.22.refs_2_ = bf16[64,2176]{1,0:T(8,128)(2,1)S(1)} collective-permute-done((bf16[64,2176]{1,0:T(8,128)(2,1)S(1)}, bf16[64,2176]{1,0:T(8,128)(2,1)S(1)}, u32[]{:S(2)}, u32[]{:S(2)}) %collective-permute-start.22) | collective-permute-done | bytes 278560 | tf_op jit(solution)/shard_map/ppermute | solution.py:249
  54.1 3.1 %collective-permute-done.30.refs_1_ = bf16[64,2176]{1,0:T(8,128)(2,1)} collective-permute-done((bf16[64,2176]{1,0:T(8,128)(2,1)S(1)}, bf16[64,2176]{1,0:T(8,128)(2,1)}, u32[]{:S(2)}, u32[]{:S(2)}) %collective-permute-start.30) | collective-permute-done | bytes 278560 | tf_op jit(solution)/shard_map/ppermute | solution.py:249
  57.2 2.0 %collective-permute-done.31.refs_2_ = bf16[64,2176]{1,0:T(8,128)(2,1)} collective-permute-done((bf16[64,2176]{1,0:T(8,128)(2,1)S(1)}, bf16[64,2176]{1,0:T(8,128)(2,1)}, u32[]{:S(2)}, u32[]{:S(2)}) %collective-permute-start.31) | collective-permute-done | bytes 278560 | tf_op jit(solution)/shard_map/ppermute | solution.py:249
  59.2 2.0 %copy-done = bf16[1,2048,896]{2,1,0:T(8,128)(2,1)S(1)} copy-done((bf16[1,2048,896]{2,1,0:T(8,128)(2,1)S(1)}, bf16[1,2048,896]{2,1,0:T(8,128)(2,1)}, u32[]{:S(2)}) %copy-start) | copy-done | bytes 3670040
  61.3 2.0 %copy-done.2 = bf16[1,2048,896]{2,1,0:T(8,128)(2,1)S(1)} copy-done((bf16[1,2048,896]{2,1,0:T(8,128)(2,1)S(1)}, bf16[1,2048,896]{2,1,0:T(8,128)(2,1)}, u32[]{:S(2)}) %copy-start.2) | copy-done | bytes 3670040
  70.0 11.8 %shard_map.76 = (bf16[256,2048]{1,0:T(8,128)(2,1)S(1)}, bf16[256,2048]{1,0:T(8,128)(2,1)S(1)}) custom-call(s32[1]{0:T(128)} %bitcast.refs_0_, bf16[64,2176]{1,0:T(8,128)(2,1)S(1)} %collective-permute-done.21.refs_1_, bf16[64,2176]{1,0:T(8,128)(2,1)S(1)} %copy-done.7, bf16[64,2176]{1,0:T(8,128)(2,1)S(1)} %copy-done.13, bf16[64,2176]{1,0:T(8,128)(2,1)S(1)} %copy-done.15, ...), custom_call_target="tpu_custom_call" | custom-call | flops 2818572288 | bytes 11010048 | tf_op jit(solution)/shard_map/pallas_call | solution.py:175
  83.4 14.1 %shard_map.75 = (bf16[256,2048]{1,0:T(8,128)(2,1)S(1)}, bf16[256,2048]{1,0:T(8,128)(2,1)}) custom-call(s32[1]{0:T(128)} %bitcast.refs_0_, bf16[64,2176]{1,0:T(8,128)(2,1)S(1)} %collective-permute-done.12.refs_1_, bf16[64,2176]{1,0:T(8,128)(2,1)S(1)} %collective-permute-done.13.refs_2_, bf16[64,2176]{1,0:T(8,128)(2,1)S(1)} %collective-permute-done.14.refs_3_, ...), custom_call_target="tpu_custom_call" | custom-call | flops 2818572288 | bytes 11010048 | tf_op jit(solution)/shard_map/pallas_call | solution.py:175
  97.5 9.7 %shard_map.77 = (bf16[128,2048]{1,0:T(8,128)(2,1)S(1)}, bf16[128,2048]{1,0:T(8,128)(2,1)S(1)}) custom-call(s32[1]{0:T(128)} %bitcast.refs_0_, bf16[64,2176]{1,0:T(8,128)(2,1)} %collective-permute-done.30.refs_1_, bf16[64,2176]{1,0:T(8,128)(2,1)} %collective-permute-done.31.refs_2_, bf16[64,2176]{1,0:T(8,128)(2,1)} %collective-permute-done.32.refs_3_, ...), custom_call_target="tpu_custom_call" | custom-call | flops 1409286144 | bytes 11010048 | tf_op jit(solution)/shard_map/pallas_call | solution.py:175
  107.7 11.8 %shard_map.74 = (bf16[256,2048]{1,0:T(8,128)(2,1)S(1)}, bf16[256,2048]{1,0:T(8,128)(2,1)S(1)}) custom-call(s32[1]{0:T(128)} %bitcast.refs_0_, bf16[64,2176]{1,0:T(8,128)(2,1)S(1)} %collective-permute-done.3.refs_1_, bf16[64,2176]{1,0:T(8,128)(2,1)S(1)} %collective-permute-done.4.refs_2_, bf16[64,2176]{1,0:T(8,128)(2,1)S(1)} %collective-permute-done.5.refs_3_, ...), custom_call_target="tpu_custom_call" | custom-call | flops 2818572288 | bytes 11010048 | tf_op jit(solution)/shard_map/pallas_call | solution.py:175
  120.2 2.4 %collective-permute-done.refs_3_ = bf16[64,2176]{1,0:T(8,128)(2,1)S(1)} collective-permute-done((bf16[64,2176]{1,0:T(8,128)(2,1)S(1)}, bf16[64,2176]{1,0:T(8,128)(2,1)S(1)}, u32[]{:S(2)}, u32[]{:S(2)}) %collective-permute-start) | collective-permute-done | bytes 278560 | tf_op jit(solution)/shard_map/ppermute | solution.py:252
  125.7 5.3 %collective-permute-done.45.refs_2_ = bf16[64,2048]{1,0:T(8,128)(2,1)S(1)} collective-permute-done((bf16[64,2048]{1,0:T(8,128)(2,1)S(1)}, bf16[64,2048]{1,0:T(8,128)(2,1)S(1)}, u32[]{:S(2)}, u32[]{:S(2)}) %collective-permute-start.45) | collective-permute-done | bytes 262176 | tf_op jit(solution)/shard_map/ppermute | solution.py:249
  135.7 8.5 %shard_map.73 = (bf16[128,2048]{1,0:T(8,128)(2,1)S(1)}, bf16[128,2048]{1,0:T(8,128)(2,1)S(1)}) custom-call(s32[1]{0:T(128)} %bitcast.refs_0_, bf16[64,2176]{1,0:T(8,128)(2,1)S(1)} %get-tuple-element.26.refs_1_, bf16[64,2176]{1,0:T(8,128)(2,1)S(1)} %get-tuple-element.25.refs_2_, bf16[64,2176]{1,0:T(8,128)(2,1)S(1)} %collective-permute-done.refs_3_, ...), custom_call_target="tpu_custom_call" | custom-call | flops 1409286144 | bytes 11010048 | tf_op jit(solution)/shard_map/pallas_call | solution.py:175
  151.3 2.8 %collective-permute-done.40.refs_2_ = bf16[64,2048]{1,0:T(8,128)(2,1)S(1)} collective-permute-done((bf16[64,2048]{1,0:T(8,128)(2,1)S(1)}, bf16[64,2048]{1,0:T(8,128)(2,1)S(1)}, u32[]{:S(2)}, u32[]{:S(2)}) %collective-permute-start.40) | collective-permute-done | bytes 262176 | tf_op jit(solution)/shard_map/ppermute | solution.py:249
  154.2 5.1 %collective-permute-done.47.refs_2_ = bf16[64,2048]{1,0:T(8,128)(2,1)S(1)} collective-permute-done((bf16[64,2048]{1,0:T(8,128)(2,1)S(1)}, bf16[64,2048]{1,0:T(8,128)(2,1)S(1)}, u32[]{:S(2)}, u32[]{:S(2)}) %collective-permute-start.47) | collective-permute-done | bytes 262176 | tf_op jit(solution)/shard_map/ppermute | solution.py:249
  163.2 5.4 %collective-permute-done.48.refs_3_ = bf16[64,2048]{1,0:T(8,128)(2,1)S(1)} collective-permute-done((bf16[64,2048]{1,0:T(8,128)(2,1)S(1)}, bf16[64,2048]{1,0:T(8,128)(2,1)S(1)}, u32[]{:S(2)}, u32[]{:S(2)}) %collective-permute-start.48) | collective-permute-done | bytes 262176 | tf_op jit(solution)/shard_map/ppermute | solution.py:249
  168.8 4.2 %collective-permute-done.41.refs_3_ = bf16[64,2048]{1,0:T(8,128)(2,1)S(1)} collective-permute-done((bf16[64,2048]{1,0:T(8,128)(2,1)S(1)}, bf16[64,2048]{1,0:T(8,128)(2,1)S(1)}, u32[]{:S(2)}, u32[]{:S(2)}) %collective-permute-start.41) | collective-permute-done | bytes 262176 | tf_op jit(solution)/shard_map/ppermute | solution.py:249
  (150 shorter events, 53.9 us)
Async XLA Ops:
  8.5 13.4 %collective-permute-start.4 = (bf16[64,2176]{1,0:T(8,128)(2,1)S(1)}, bf16[64,2176]{1,0:T(8,128)(2,1)S(1)}, u32[]{:S(2)}, u32[]{:S(2)}) collective-permute-start(bf16[64,2176]{1,0:T(8,128)(2,1)S(1)} %get-tuple-element.25.refs_2_), channel_id=1, source_target_pairs={{0,4},{4,8},{8,12},{12,14},{14,10},{10,6},{6,2},{2,0},{1,5},{5,9},... | collective-permute-start | bytes 835592 | tf_op jit(solution)/shard_map/ppermute | solution.py:249
  10.1 13.9 %collective-permute-start.7 = (bf16[64,2176]{1,0:T(8,128)(2,1)S(1)}, bf16[64,2176]{1,0:T(8,128)(2,1)S(1)}, u32[]{:S(2)}, u32[]{:S(2)}) collective-permute-start(bf16[64,2176]{1,0:T(8,128)(2,1)S(1)} %get-tuple-element.26.refs_1_), channel_id=1, source_target_pairs={{4,0},{8,4},{12,8},{14,12},{10,14},{6,10},{2,6},{0,2},{5,1},{9,5},... | collective-permute-start | bytes 835592 | tf_op jit(solution)/shard_map/ppermute | solution.py:249
  10.5 13.5 %collective-permute-start.8 = (bf16[64,2176]{1,0:T(8,128)(2,1)S(1)}, bf16[64,2176]{1,0:T(8,128)(2,1)S(1)}, u32[]{:S(2)}, u32[]{:S(2)}) collective-permute-start(bf16[64,2176]{1,0:T(8,128)(2,1)S(1)} %get-tuple-element.25.refs_2_), channel_id=1, source_target_pairs={{4,0},{8,4},{12,8},{14,12},{10,14},{6,10},{2,6},{0,2},{5,1},{9,5},... | collective-permute-start | bytes 835592 | tf_op jit(solution)/shard_map/ppermute | solution.py:249
  24.0 11.9 %collective-permute-start.16 = (bf16[64,2176]{1,0:T(8,128)(2,1)S(1)}, bf16[64,2176]{1,0:T(8,128)(2,1)S(1)}, u32[]{:S(2)}, u32[]{:S(2)}) collective-permute-start(bf16[64,2176]{1,0:T(8,128)(2,1)S(1)} %collective-permute-done.7.refs_5_), channel_id=1, source_target_pairs={{4,0},{8,4},{12,8},{14,12},{10,14},{6,10},{2,6},{0,2},{5,1},{9,5},... | collective-permute-start | bytes 835592 | tf_op jit(solution)/shard_map/ppermute | solution.py:249
  24.0 12.1 %collective-permute-start.17 = (bf16[64,2176]{1,0:T(8,128)(2,1)S(1)}, bf16[64,2176]{1,0:T(8,128)(2,1)S(1)}, u32[]{:S(2)}, u32[]{:S(2)}) collective-permute-start(bf16[64,2176]{1,0:T(8,128)(2,1)S(1)} %collective-permute-done.8.refs_6_), channel_id=1, source_target_pairs={{4,0},{8,4},{12,8},{14,12},{10,14},{6,10},{2,6},{0,2},{5,1},{9,5},... | collective-permute-start | bytes 835592 | tf_op jit(solution)/shard_map/ppermute | solution.py:249
  52.2 29.5 %collective-permute-start.15 = (bf16[64,2176]{1,0:T(8,128)(2,1)S(1)}, bf16[64,2176]{1,0:T(8,128)(2,1)}, u32[]{:S(2)}, u32[]{:S(2)}) collective-permute-start(bf16[64,2176]{1,0:T(8,128)(2,1)S(1)} %collective-permute-done.13.refs_2_), channel_id=1, source_target_pairs={{0,1},{1,0},{2,3},{3,2},{4,5},{5,4},{6,7},{7,6},{8,9},{9,8},{10,11... | collective-permute-start | bytes 835592 | tf_op jit(solution)/shard_map/ppermute | solution.py:252
  52.9 29.4 %collective-permute-start.18 = (bf16[64,2176]{1,0:T(8,128)(2,1)S(1)}, bf16[64,2176]{1,0:T(8,128)(2,1)}, u32[]{:S(2)}, u32[]{:S(2)}) collective-permute-start(bf16[64,2176]{1,0:T(8,128)(2,1)S(1)} %collective-permute-done.16.refs_5_), channel_id=1, source_target_pairs={{0,1},{1,0},{2,3},{3,2},{4,5},{5,4},{6,7},{7,6},{8,9},{9,8},{10,11... | collective-permute-start | bytes 835592 | tf_op jit(solution)/shard_map/ppermute | solution.py:252
  54.1 28.3 %collective-permute-start.19 = (bf16[64,2176]{1,0:T(8,128)(2,1)S(1)}, bf16[64,2176]{1,0:T(8,128)(2,1)}, u32[]{:S(2)}, u32[]{:S(2)}) collective-permute-start(bf16[64,2176]{1,0:T(8,128)(2,1)S(1)} %collective-permute-done.17.refs_6_), channel_id=1, source_target_pairs={{0,1},{1,0},{2,3},{3,2},{4,5},{5,4},{6,7},{7,6},{8,9},{9,8},{10,11... | collective-permute-start | bytes 835592 | tf_op jit(solution)/shard_map/ppermute | solution.py:252
  57.2 25.7 %collective-permute-start.32 = (bf16[64,2176]{1,0:T(8,128)(2,1)}, bf16[64,2176]{1,0:T(8,128)(2,1)}, u32[]{:S(2)}, u32[]{:S(2)}) collective-permute-start(bf16[64,2176]{1,0:T(8,128)(2,1)} %collective-permute-done.30.refs_1_), channel_id=1, source_target_pairs={{0,1},{1,0},{2,3},{3,2},{4,5},{5,4},{6,7},{7,6},{8,9},{9,8},{10,11... | collective-permute-start | bytes 835592 | tf_op jit(solution)/shard_map/ppermute | solution.py:252
  59.2 23.7 %collective-permute-start.33 = (bf16[64,2176]{1,0:T(8,128)(2,1)}, bf16[64,2176]{1,0:T(8,128)(2,1)}, u32[]{:S(2)}, u32[]{:S(2)}) collective-permute-start(bf16[64,2176]{1,0:T(8,128)(2,1)} %collective-permute-done.31.refs_2_), channel_id=1, source_target_pairs={{0,1},{1,0},{2,3},{3,2},{4,5},{5,4},{6,7},{7,6},{8,9},{9,8},{10,11... | collective-permute-start | bytes 835592 | tf_op jit(solution)/shard_map/ppermute | solution.py:252
  81.8 25.4 %collective-permute-start.5 = (bf16[64,2176]{1,0:T(8,128)(2,1)S(1)}, bf16[64,2176]{1,0:T(8,128)(2,1)S(1)}, u32[]{:S(2)}, u32[]{:S(2)}) collective-permute-start(bf16[64,2176]{1,0:T(8,128)(2,1)S(1)} %collective-permute-done.3.refs_1_), channel_id=1, source_target_pairs={{0,1},{1,0},{2,3},{3,2},{4,5},{5,4},{6,7},{7,6},{8,9},{9,8},{10,11... | collective-permute-start | bytes 835592 | tf_op jit(solution)/shard_map/ppermute | solution.py:252
  82.3 24.9 %collective-permute-start.6 = (bf16[64,2176]{1,0:T(8,128)(2,1)S(1)}, bf16[64,2176]{1,0:T(8,128)(2,1)S(1)}, u32[]{:S(2)}, u32[]{:S(2)}) collective-permute-start(bf16[64,2176]{1,0:T(8,128)(2,1)S(1)} %collective-permute-done.4.refs_2_), channel_id=1, source_target_pairs={{0,1},{1,0},{2,3},{3,2},{4,5},{5,4},{6,7},{7,6},{8,9},{9,8},{10,11... | collective-permute-start | bytes 835592 | tf_op jit(solution)/shard_map/ppermute | solution.py:252
  82.4 25.3 %collective-permute-start.9 = (bf16[64,2176]{1,0:T(8,128)(2,1)S(1)}, bf16[64,2176]{1,0:T(8,128)(2,1)S(1)}, u32[]{:S(2)}, u32[]{:S(2)}) collective-permute-start(bf16[64,2176]{1,0:T(8,128)(2,1)S(1)} %collective-permute-done.7.refs_5_), channel_id=1, source_target_pairs={{0,1},{1,0},{2,3},{3,2},{4,5},{5,4},{6,7},{7,6},{8,9},{9,8},{10,11... | collective-permute-start | bytes 835592 | tf_op jit(solution)/shard_map/ppermute | solution.py:252
  82.9 24.9 %collective-permute-start.10 = (bf16[64,2176]{1,0:T(8,128)(2,1)S(1)}, bf16[64,2176]{1,0:T(8,128)(2,1)S(1)}, u32[]{:S(2)}, u32[]{:S(2)}) collective-permute-start(bf16[64,2176]{1,0:T(8,128)(2,1)S(1)} %collective-permute-done.8.refs_6_), channel_id=1, source_target_pairs={{0,1},{1,0},{2,3},{3,2},{4,5},{5,4},{6,7},{7,6},{8,9},{9,8},{10,11... | collective-permute-start | bytes 835592 | tf_op jit(solution)/shard_map/ppermute | solution.py:252
  83.0 41.3 %collective-permute-start.29 = (bf16[256,2048]{1,0:T(8,128)(2,1)S(1)}, bf16[256,2048]{1,0:T(8,128)(2,1)S(1)}, u32[]{:S(2)}, u32[]{:S(2)}) collective-permute-start(bf16[256,2048]{1,0:T(8,128)(2,1)S(1)} %get-tuple-element.22), channel_id=1, source_target_pairs={{0,1},{1,0},{2,3},{3,2},{4,5},{5,4},{6,7},{7,6},{8,9},{9,8},{10,11... | collective-permute-start | bytes 3145736 | tf_op jit(solution)/shard_map/ppermute | solution.py:252
  107.1 28.0 %collective-permute-start.20 = (bf16[256,2048]{1,0:T(8,128)(2,1)}, bf16[256,2048]{1,0:T(8,128)(2,1)S(1)}, u32[]{:S(2)}, u32[]{:S(2)}) collective-permute-start(bf16[256,2048]{1,0:T(8,128)(2,1)} %get-tuple-element.20), channel_id=1, source_target_pairs={{0,1},{1,0},{2,3},{3,2},{4,5},{5,4},{6,7},{7,6},{8,9},{9,8},{10,11... | collective-permute-start | bytes 3145736 | tf_op jit(solution)/shard_map/ppermute | solution.py:252
  107.2 12.9 %collective-permute-start.34 = (bf16[128,2048]{1,0:T(8,128)(2,1)S(1)}, bf16[128,2048]{1,0:T(8,128)(2,1)S(1)}, u32[]{:S(2)}, u32[]{:S(2)}) collective-permute-start(bf16[128,2048]{1,0:T(8,128)(2,1)S(1)} %get-tuple-element.24), channel_id=1, source_target_pairs={{0,1},{1,0},{2,3},{3,2},{4,5},{5,4},{6,7},{7,6},{8,9},{9,8},{10,11... | collective-permute-start | bytes 1572872 | tf_op jit(solution)/shard_map/ppermute | solution.py:252
  119.5 28.8 %collective-permute-start.11 = (bf16[256,2048]{1,0:T(8,128)(2,1)S(1)}, bf16[256,2048]{1,0:T(8,128)(2,1)S(1)}, u32[]{:S(2)}, u32[]{:S(2)}) collective-permute-start(bf16[256,2048]{1,0:T(8,128)(2,1)S(1)} %get-tuple-element.18), channel_id=1, source_target_pairs={{0,1},{1,0},{2,3},{3,2},{4,5},{5,4},{6,7},{7,6},{8,9},{9,8},{10,11... | collective-permute-start | bytes 3145736 | tf_op jit(solution)/shard_map/ppermute | solution.py:252
  124.9 19.3 %collective-permute-start.42 = (bf16[64,2048]{1,0:T(8,128)(2,1)S(1)}, bf16[64,2048]{1,0:T(8,128)(2,1)S(1)}, u32[]{:S(2)}, u32[]{:S(2)}) collective-permute-start(bf16[64,2048]{1,0:T(8,128)(2,1)S(1)} %shard_map.86), channel_id=1, source_target_pairs={{4,0},{8,4},{12,8},{14,12},{10,14},{6,10},{2,6},{0,2},{5,1},{9,5},... | collective-permute-start | bytes 786440 | tf_op jit(solution)/shard_map/ppermute | solution.py:249
  131.0 13.8 %collective-permute-start.39 = (bf16[64,2048]{1,0:T(8,128)(2,1)S(1)}, bf16[64,2048]{1,0:T(8,128)(2,1)S(1)}, u32[]{:S(2)}, u32[]{:S(2)}) collective-permute-start(bf16[64,2048]{1,0:T(8,128)(2,1)S(1)} %shard_map.82), channel_id=1, source_target_pairs={{0,4},{4,8},{8,12},{12,14},{14,10},{10,6},{6,2},{2,0},{1,5},{5,9},... | collective-permute-start | bytes 786440 | tf_op jit(solution)/shard_map/ppermute | solution.py:249
  144.8 18.4 %collective-permute-start.2 = (bf16[128,2048]{1,0:T(8,128)(2,1)S(1)}, bf16[128,2048]{1,0:T(8,128)(2,1)S(1)}, u32[]{:S(2)}, u32[]{:S(2)}) collective-permute-start(bf16[128,2048]{1,0:T(8,128)(2,1)S(1)} %get-tuple-element.16), channel_id=1, source_target_pairs={{0,1},{1,0},{2,3},{3,2},{4,5},{5,4},{6,7},{7,6},{8,9},{9,8},{10,11... | collective-permute-start | bytes 1572872 | tf_op jit(solution)/shard_map/ppermute | solution.py:252
  146.6 12.6 %collective-permute-start.47 = (bf16[64,2048]{1,0:T(8,128)(2,1)S(1)}, bf16[64,2048]{1,0:T(8,128)(2,1)S(1)}, u32[]{:S(2)}, u32[]{:S(2)}) collective-permute-start(bf16[64,2048]{1,0:T(8,128)(2,1)S(1)} %shard_map.91), channel_id=1, source_target_pairs={{0,4},{4,8},{8,12},{12,14},{14,10},{10,6},{6,2},{2,0},{1,5},{5,9},... | collective-permute-start | bytes 786440 | tf_op jit(solution)/shard_map/ppermute | solution.py:249
  148.3 14.2 %collective-permute-start.37 = (bf16[64,2048]{1,0:T(8,128)(2,1)S(1)}, bf16[64,2048]{1,0:T(8,128)(2,1)S(1)}, u32[]{:S(2)}, u32[]{:S(2)}) collective-permute-start(bf16[64,2048]{1,0:T(8,128)(2,1)S(1)} %shard_map.80), channel_id=1, source_target_pairs={{4,0},{8,4},{12,8},{14,12},{10,14},{6,10},{2,6},{0,2},{5,1},{9,5},... | collective-permute-start | bytes 786440 | tf_op jit(solution)/shard_map/ppermute | solution.py:249
  150.8 12.4 %collective-permute-start.44 = (bf16[64,2048]{1,0:T(8,128)(2,1)S(1)}, bf16[64,2048]{1,0:T(8,128)(2,1)S(1)}, u32[]{:S(2)}, u32[]{:S(2)}) collective-permute-start(bf16[64,2048]{1,0:T(8,128)(2,1)S(1)} %shard_map.88), channel_id=1, source_target_pairs={{4,0},{8,4},{12,8},{14,12},{10,14},{6,10},{2,6},{0,2},{5,1},{9,5},... | collective-permute-start | bytes 786440 | tf_op jit(solution)/shard_map/ppermute | solution.py:249
  (45 other events, 294.4 us)
where the time goes:
time: 174 us
  Pallas kernels  57.2 us (33%)
  waiting for transfers between devices  56.4 us (32%)
  starting transfers between devices  38.1 us (22%)
  local copies, waits for them, and re-layouts  16.4 us (9%)
  other arithmetic  5.52 us (3%)
    pallas_call x5, Pallas kernels, expert_blocks(): pl.pallas_call(functools.partial(expert_kernel, tok_rows, capacity, exper...  55.7 us
    ppermute x28, waiting for transfers between devices, shift(): return lax.ppermute(value, 'ep', pairs)  54 us
    ppermute x28, starting transfers between devices, shift(): return lax.ppermute(value, 'ep', pairs)  34.2 us
    unnamed x40, local copies, waits for them, and re-layouts  15.8 us
    ppermute x21, starting transfers between devices, other(): return lax.ppermute(value, 'tp', swap)  3.86 us
  transfers between devices with their start and end apart: 49, of which 18 were waited for; matrix products, arithmetic and copies ran while one was open for 0% of the time, Pallas kernels for 33%

commit v1 on v0

--- a/solution.py
+++ b/solution.py
@@ -75,32 +75,12 @@
     number = pairs * 2 * pieces
     which = refs[0]
     blocks = refs[1 : 1 + number]
-    gate_hbm, up_hbm, down_hbm, own_out, other_out = refs[1 + number : 6 + number]
-    gate_mat, up_mat, down_mat, chosen, hidden, weight, spread, gather, sems = refs[6 + number :]
-    feat_width, hid_width = gate_mat.shape
+    gate_mat, up_mat, down_mat, own_out, other_out = refs[1 + number : 6 + number]
+    chosen, hidden, weight, spread, gather = refs[6 + number :]
+    feat_width, hid_width = gate_mat.shape[1:]
     tile = 256
     hid_tiles, out_tiles = hid_width // tile, feat_width // tile
     tail = hid_width - hid_tiles * tile
-
-    def hid_copy(i, at, width):
-        cols = pl.ds(at, width)
-        return (
-            pltpu.make_async_copy(gate_hbm.at[0, :, cols], gate_mat.at[:, cols], sems.at[0, i]),
-            pltpu.make_async_copy(up_hbm.at[0, :, cols], up_mat.at[:, cols], sems.at[1, i]),
-        )
-
-    def out_copy(i, at):
-        cols = pl.ds(at, tile)
-        return pltpu.make_async_copy(down_hbm.at[0, :, cols], down_mat.at[:, cols], sems.at[2, i])
-
-    for i in range(hid_tiles):
-        for copy in hid_copy(i, i * tile, tile):
-            copy.start()
-    if tail:
-        for copy in hid_copy(hid_tiles, hid_tiles * tile, tail):
-            copy.start()
-    for i in range(out_tiles):
-        out_copy(i, i * tile).start()
 
     tokens, slots = 2 * tok_rows, 2 * capacity
     row = lax.broadcasted_iota(jnp.int32, (tokens, tokens), 0)
@@ -130,12 +110,10 @@
             picked = jnp.dot(gather[p], part, preferred_element_type=jnp.float32)
             chosen[p * slots : (p + 1) * slots, cols] = picked.astype(jnp.bfloat16)
 
-    def hid_tile(i, at, width):
-        for copy in hid_copy(i, at, width):
-            copy.wait()
+    def hid_tile(at, width):
         cols = pl.ds(at, width)
-        gate_pre = jnp.dot(chosen[...], gate_mat[:, cols], preferred_element_type=jnp.float32)
-        up_pre = jnp.dot(chosen[...], up_mat[:, cols], preferred_element_type=jnp.float32)
+        gate_pre = jnp.dot(chosen[...], gate_mat[0, :, cols], preferred_element_type=jnp.float32)
+        up_pre = jnp.dot(chosen[...], up_mat[0, :, cols], preferred_element_type=jnp.float32)
         gated = jnp.minimum(gate_pre, clamp_limit)
         upper = jnp.clip(up_pre, -clamp_limit, clamp_limit)
         value = gated * jax.nn.sigmoid(sig_alpha * gated) * (upper + 1.0)
@@ -143,17 +121,16 @@
 
     @pl.loop(0, hid_tiles)
     def _(i):
-        hid_tile(i, pl.multiple_of(i * tile, tile), tile)
+        hid_tile(pl.multiple_of(i * tile, tile), tile)
 
     if tail:
-        hid_tile(hid_tiles, hid_tiles * tile, tail)
+        hid_tile(hid_tiles * tile, tail)
 
     @pl.loop(0, out_tiles)
     def _(i):
         at = pl.multiple_of(i * tile, tile)
-        out_copy(i, at).wait()
         cols = pl.ds(at, tile)
-        out = jnp.dot(hidden[...], down_mat[:, cols], preferred_element_type=jnp.float32)
+        out = jnp.dot(hidden[...], down_mat[0, :, cols], preferred_element_type=jnp.float32)
         out = out.astype(jnp.bfloat16)
         for p in range(pairs):
             full = jnp.dot(
@@ -177,20 +154,16 @@
         out_shape=(shape, shape),
         in_specs=[pl.BlockSpec(memory_space=pltpu.SMEM)]
         + [vmem] * len(flat)
-        + [pl.BlockSpec(memory_space=pltpu.HBM)] * 3,
+        + [vmem] * 3,
         out_specs=(vmem, vmem),
         scratch_shapes=[
-            pltpu.VMEM((feat_width, hid_width), jnp.bfloat16),
-            pltpu.VMEM((feat_width, hid_width), jnp.bfloat16),
-            pltpu.VMEM((hid_width, feat_width), jnp.bfloat16),
             pltpu.VMEM((rows, feat_width), jnp.bfloat16),
             pltpu.VMEM((rows, hid_width), jnp.bfloat16),
             pltpu.VMEM((pairs, tokens, 256), jnp.float32),
             pltpu.VMEM((pairs, tokens, slots), jnp.bfloat16),
             pltpu.VMEM((pairs, slots, tokens), jnp.bfloat16),
-            pltpu.SemaphoreType.DMA((3, 8)),
         ],
-        compiler_params=pltpu.CompilerParams(vmem_limit_bytes=40 * 2**20),
+        compiler_params=pltpu.CompilerParams(vmem_limit_bytes=26 * 2**20),
         cost_estimate=pl.CostEstimate(
             flops=6 * rows * feat_width * hid_width,
             bytes_accessed=6 * feat_width * hid_width,

time: 174 us -> 170 us (0.977)
  Pallas kernels: 57.2 us -> 51.1 us
  local copies, waits for them, and re-layouts: 16.4 us -> 18.4 us
    pallas_call x5, Pallas kernels: 55.7 us -> 49.6 us  [expert_blocks(): pl.pallas_call(functools.partial(expert_kernel, tok_rows, capacity, exper...]
    unnamed x40, local copies, waits for them, and re-layouts: 15.8 us -> 17.8 us
  transfers between devices with their start and end apart: 49 -> 49, of which waited for: 18 -> 19; matrix products, arithmetic and copies ran while one was open for 0% -> 0% of each run, Pallas kernels for 33% -> 30%
where the time goes in v1:
time: 170 us; the launch traced here: 169 us
  waiting for transfers between devices  56.3 us (33%)
  Pallas kernels  51.1 us (30%)
  starting transfers between devices  37.8 us (22%)
  local copies, waits for them, and re-layouts  18.4 us (11%)
  other arithmetic  5.52 us (3%)
    ppermute x28, waiting for transfers between devices, shift(): return lax.ppermute(value, 'ep', pairs)  53.9 us
    pallas_call x5, Pallas kernels, expert_blocks(): pl.pallas_call(functools.partial(expert_kernel, tok_rows, capacity, exper...  49.6 us
    ppermute x28, starting transfers between devices, shift(): return lax.ppermute(value, 'ep', pairs)  33.9 us
    unnamed x40, local copies, waits for them, and re-layouts  17.8 us
    ppermute x21, starting transfers between devices, other(): return lax.ppermute(value, 'tp', swap)  3.86 us
  transfers between devices with their start and end apart: 49, of which 19 were waited for; matrix products, arithmetic and copies ran while one was open for 0% of the time, Pallas kernels for 30%

profile of v1, /device:TPU:0, one launch (start us, length us, event | category | flops | bytes accessed | tf_op | source)
XLA Modules:
  0.0 169.4 jit_solution(8167476918917086635)
XLA Ops:
  5.4 3.1 %collective-permute-start.3 = (bf16[64,2176]{1,0:T(8,128)(2,1)S(1)}, bf16[64,2176]{1,0:T(8,128)(2,1)S(1)}, u32[]{:S(2)}, u32[]{:S(2)}) collective-permute-start(bf16[64,2176]{1,0:T(8,128)(2,1)S(1)} %get-tuple-element.26.refs_1_), channel_id=1, source_target_pairs={{0,4},{4,8},{8,12},{12,14},{14,10},{10,6},{6,2},{2,0},{1,5},{5,9},... | collective-permute-start | bytes 835592 | tf_op jit(solution)/shard_map/ppermute | solution.py:222
  10.5 5.4 %collective-permute-done.3.refs_1_ = bf16[64,2176]{1,0:T(8,128)(2,1)S(1)} collective-permute-done((bf16[64,2176]{1,0:T(8,128)(2,1)S(1)}, bf16[64,2176]{1,0:T(8,128)(2,1)S(1)}, u32[]{:S(2)}, u32[]{:S(2)}) %collective-permute-start.3) | collective-permute-done | bytes 278560 | tf_op jit(solution)/shard_map/ppermute | solution.py:222
  15.9 2.1 %collective-permute-start.12 = (bf16[64,2176]{1,0:T(8,128)(2,1)S(1)}, bf16[64,2176]{1,0:T(8,128)(2,1)S(1)}, u32[]{:S(2)}, u32[]{:S(2)}) collective-permute-start(bf16[64,2176]{1,0:T(8,128)(2,1)S(1)} %collective-permute-done.3.refs_1_), channel_id=1, source_target_pairs={{0,4},{4,8},{8,12},{12,14},{14,10},{10,6},{6,2},{2,0},{1,5},{5,9},... | collective-permute-start | bytes 835592 | tf_op jit(solution)/shard_map/ppermute | solution.py:222
  18.0 3.9 %collective-permute-done.4.refs_2_ = bf16[64,2176]{1,0:T(8,128)(2,1)S(1)} collective-permute-done((bf16[64,2176]{1,0:T(8,128)(2,1)S(1)}, bf16[64,2176]{1,0:T(8,128)(2,1)S(1)}, u32[]{:S(2)}, u32[]{:S(2)}) %collective-permute-start.4) | collective-permute-done | bytes 278560 | tf_op jit(solution)/shard_map/ppermute | solution.py:222
  21.9 2.1 %collective-permute-start.13 = (bf16[64,2176]{1,0:T(8,128)(2,1)S(1)}, bf16[64,2176]{1,0:T(8,128)(2,1)S(1)}, u32[]{:S(2)}, u32[]{:S(2)}) collective-permute-start(bf16[64,2176]{1,0:T(8,128)(2,1)S(1)} %collective-permute-done.4.refs_2_), channel_id=1, source_target_pairs={{0,4},{4,8},{8,12},{12,14},{14,10},{10,6},{6,2},{2,0},{1,5},{5,9},... | collective-permute-start | bytes 835592 | tf_op jit(solution)/shard_map/ppermute | solution.py:222
  27.9 2.1 %collective-permute-start.21 = (bf16[64,2176]{1,0:T(8,128)(2,1)S(1)}, bf16[64,2176]{1,0:T(8,128)(2,1)S(1)}, u32[]{:S(2)}, u32[]{:S(2)}) collective-permute-start(bf16[64,2176]{1,0:T(8,128)(2,1)S(1)} %collective-permute-done.12.refs_1_), channel_id=1, source_target_pairs={{0,4},{4,8},{8,12},{12,14},{14,10},{10,6},{6,2},{2,0},{1,5},{5,9},... | collective-permute-start | bytes 835592 | tf_op jit(solution)/shard_map/ppermute | solution.py:222
  29.9 3.9 %collective-permute-done.13.refs_2_ = bf16[64,2176]{1,0:T(8,128)(2,1)S(1)} collective-permute-done((bf16[64,2176]{1,0:T(8,128)(2,1)S(1)}, bf16[64,2176]{1,0:T(8,128)(2,1)S(1)}, u32[]{:S(2)}, u32[]{:S(2)}) %collective-permute-start.13) | collective-permute-done | bytes 278560 | tf_op jit(solution)/shard_map/ppermute | solution.py:222
  33.8 2.1 %collective-permute-start.22 = (bf16[64,2176]{1,0:T(8,128)(2,1)S(1)}, bf16[64,2176]{1,0:T(8,128)(2,1)S(1)}, u32[]{:S(2)}, u32[]{:S(2)}) collective-permute-start(bf16[64,2176]{1,0:T(8,128)(2,1)S(1)} %collective-permute-done.13.refs_2_), channel_id=1, source_target_pairs={{0,4},{4,8},{8,12},{12,14},{14,10},{10,6},{6,2},{2,0},{1,5},{5,9},... | collective-permute-start | bytes 835592 | tf_op jit(solution)/shard_map/ppermute | solution.py:222
  39.8 5.1 %collective-permute-done.22.refs_2_ = bf16[64,2176]{1,0:T(8,128)(2,1)S(1)} collective-permute-done((bf16[64,2176]{1,0:T(8,128)(2,1)S(1)}, bf16[64,2176]{1,0:T(8,128)(2,1)S(1)}, u32[]{:S(2)}, u32[]{:S(2)}) %collective-permute-start.22) | collective-permute-done | bytes 278560 | tf_op jit(solution)/shard_map/ppermute | solution.py:222
  54.1 3.1 %collective-permute-done.30.refs_1_ = bf16[64,2176]{1,0:T(8,128)(2,1)} collective-permute-done((bf16[64,2176]{1,0:T(8,128)(2,1)S(1)}, bf16[64,2176]{1,0:T(8,128)(2,1)}, u32[]{:S(2)}, u32[]{:S(2)}) %collective-permute-start.30) | collective-permute-done | bytes 278560 | tf_op jit(solution)/shard_map/ppermute | solution.py:222
  59.2 2.0 %copy-done = bf16[1,2048,896]{2,1,0:T(8,128)(2,1)S(1)} copy-done((bf16[1,2048,896]{2,1,0:T(8,128)(2,1)S(1)}, bf16[1,2048,896]{2,1,0:T(8,128)(2,1)}, u32[]{:S(2)}) %copy-start) | copy-done | bytes 3670040
  61.3 2.0 %copy-done.2 = bf16[1,2048,896]{2,1,0:T(8,128)(2,1)S(1)} copy-done((bf16[1,2048,896]{2,1,0:T(8,128)(2,1)S(1)}, bf16[1,2048,896]{2,1,0:T(8,128)(2,1)}, u32[]{:S(2)}) %copy-start.2) | copy-done | bytes 3670040
  63.3 2.0 %copy-done.4 = bf16[1,896,2048]{2,1,0:T(8,128)(2,1)S(1)} copy-done((bf16[1,896,2048]{2,1,0:T(8,128)(2,1)S(1)}, bf16[1,896,2048]{2,1,0:T(8,128)(2,1)}, u32[]{:S(2)}) %copy-start.4) | copy-done | bytes 3670040
  72.0 11.0 %shard_map.76 = (bf16[256,2048]{1,0:T(8,128)(2,1)S(1)}, bf16[256,2048]{1,0:T(8,128)(2,1)S(1)}) custom-call(s32[1]{0:T(128)} %bitcast.refs_0_, bf16[64,2176]{1,0:T(8,128)(2,1)S(1)} %collective-permute-done.21.refs_1_, bf16[64,2176]{1,0:T(8,128)(2,1)S(1)} %copy-done.7, bf16[64,2176]{1,0:T(8,128)(2,1)S(1)} %copy-done.13, bf16[64,2176]{1,0:T(8,128)(2,1)S(1)} %copy-done.15, ...), custom_call_target="tpu_custom_call" | custom-call | flops 2818572288 | bytes 11010048 | tf_op jit(solution)/shard_map/pallas_call | solution.py:152
  84.6 12.1 %shard_map.75 = (bf16[256,2048]{1,0:T(8,128)(2,1)S(1)}, bf16[256,2048]{1,0:T(8,128)(2,1)S(1)}) custom-call(s32[1]{0:T(128)} %bitcast.refs_0_, bf16[64,2176]{1,0:T(8,128)(2,1)S(1)} %collective-permute-done.12.refs_1_, bf16[64,2176]{1,0:T(8,128)(2,1)S(1)} %collective-permute-done.13.refs_2_, bf16[64,2176]{1,0:T(8,128)(2,1)S(1)} %collective-permute-done.14.refs_3_, ...), custom_call_target="tpu_custom_call" | custom-call | flops 2818572288 | bytes 11010048 | tf_op jit(solution)/shard_map/pallas_call | solution.py:152
  96.7 8.4 %shard_map.77 = (bf16[128,2048]{1,0:T(8,128)(2,1)S(1)}, bf16[128,2048]{1,0:T(8,128)(2,1)S(1)}) custom-call(s32[1]{0:T(128)} %bitcast.refs_0_, bf16[64,2176]{1,0:T(8,128)(2,1)} %collective-permute-done.30.refs_1_, bf16[64,2176]{1,0:T(8,128)(2,1)} %collective-permute-done.31.refs_2_, bf16[64,2176]{1,0:T(8,128)(2,1)} %collective-permute-done.32.refs_3_, ...), custom_call_target="tpu_custom_call" | custom-call | flops 1409286144 | bytes 11010048 | tf_op jit(solution)/shard_map/pallas_call | solution.py:152
  105.7 11.0 %shard_map.74 = (bf16[256,2048]{1,0:T(8,128)(2,1)S(1)}, bf16[256,2048]{1,0:T(8,128)(2,1)S(1)}) custom-call(s32[1]{0:T(128)} %bitcast.refs_0_, bf16[64,2176]{1,0:T(8,128)(2,1)S(1)} %collective-permute-done.3.refs_1_, bf16[64,2176]{1,0:T(8,128)(2,1)S(1)} %collective-permute-done.4.refs_2_, bf16[64,2176]{1,0:T(8,128)(2,1)S(1)} %collective-permute-done.5.refs_3_, ...), custom_call_target="tpu_custom_call" | custom-call | flops 2818572288 | bytes 11010048 | tf_op jit(solution)/shard_map/pallas_call | solution.py:152
  117.4 2.4 %collective-permute-done.refs_3_ = bf16[64,2176]{1,0:T(8,128)(2,1)S(1)} collective-permute-done((bf16[64,2176]{1,0:T(8,128)(2,1)S(1)}, bf16[64,2176]{1,0:T(8,128)(2,1)S(1)}, u32[]{:S(2)}, u32[]{:S(2)}) %collective-permute-start) | collective-permute-done | bytes 278560 | tf_op jit(solution)/shard_map/ppermute | solution.py:225
  122.6 5.5 %collective-permute-done.45.refs_2_ = bf16[64,2048]{1,0:T(8,128)(2,1)S(1)} collective-permute-done((bf16[64,2048]{1,0:T(8,128)(2,1)S(1)}, bf16[64,2048]{1,0:T(8,128)(2,1)S(1)}, u32[]{:S(2)}, u32[]{:S(2)}) %collective-permute-start.45) | collective-permute-done | bytes 262176 | tf_op jit(solution)/shard_map/ppermute | solution.py:222
  132.9 7.2 %shard_map.73 = (bf16[128,2048]{1,0:T(8,128)(2,1)S(1)}, bf16[128,2048]{1,0:T(8,128)(2,1)S(1)}) custom-call(s32[1]{0:T(128)} %bitcast.refs_0_, bf16[64,2176]{1,0:T(8,128)(2,1)S(1)} %get-tuple-element.26.refs_1_, bf16[64,2176]{1,0:T(8,128)(2,1)S(1)} %get-tuple-element.25.refs_2_, bf16[64,2176]{1,0:T(8,128)(2,1)S(1)} %collective-permute-done.refs_3_, ...), custom_call_target="tpu_custom_call" | custom-call | flops 1409286144 | bytes 11010048 | tf_op jit(solution)/shard_map/pallas_call | solution.py:152
  147.2 3.2 %collective-permute-done.40.refs_2_ = bf16[64,2048]{1,0:T(8,128)(2,1)S(1)} collective-permute-done((bf16[64,2048]{1,0:T(8,128)(2,1)S(1)}, bf16[64,2048]{1,0:T(8,128)(2,1)S(1)}, u32[]{:S(2)}, u32[]{:S(2)}) %collective-permute-start.40) | collective-permute-done | bytes 262176 | tf_op jit(solution)/shard_map/ppermute | solution.py:222
  150.5 4.7 %collective-permute-done.47.refs_2_ = bf16[64,2048]{1,0:T(8,128)(2,1)S(1)} collective-permute-done((bf16[64,2048]{1,0:T(8,128)(2,1)S(1)}, bf16[64,2048]{1,0:T(8,128)(2,1)S(1)}, u32[]{:S(2)}, u32[]{:S(2)}) %collective-permute-start.47) | collective-permute-done | bytes 262176 | tf_op jit(solution)/shard_map/ppermute | solution.py:222
  159.1 5.4 %collective-permute-done.48.refs_3_ = bf16[64,2048]{1,0:T(8,128)(2,1)S(1)} collective-permute-done((bf16[64,2048]{1,0:T(8,128)(2,1)S(1)}, bf16[64,2048]{1,0:T(8,128)(2,1)S(1)}, u32[]{:S(2)}, u32[]{:S(2)}) %collective-permute-start.48) | collective-permute-done | bytes 262176 | tf_op jit(solution)/shard_map/ppermute | solution.py:222
  164.6 3.8 %collective-permute-done.41.refs_3_ = bf16[64,2048]{1,0:T(8,128)(2,1)S(1)} collective-permute-done((bf16[64,2048]{1,0:T(8,128)(2,1)S(1)}, bf16[64,2048]{1,0:T(8,128)(2,1)S(1)}, u32[]{:S(2)}, u32[]{:S(2)}) %collective-permute-start.41) | collective-permute-done | bytes 262176 | tf_op jit(solution)/shard_map/ppermute | solution.py:222
  (150 shorter events, 55.7 us)
Async XLA Ops:
  8.5 13.4 %collective-permute-start.4 = (bf16[64,2176]{1,0:T(8,128)(2,1)S(1)}, bf16[64,2176]{1,0:T(8,128)(2,1)S(1)}, u32[]{:S(2)}, u32[]{:S(2)}) collective-permute-start(bf16[64,2176]{1,0:T(8,128)(2,1)S(1)} %get-tuple-element.25.refs_2_), channel_id=1, source_target_pairs={{0,4},{4,8},{8,12},{12,14},{14,10},{10,6},{6,2},{2,0},{1,5},{5,9},... | collective-permute-start | bytes 835592 | tf_op jit(solution)/shard_map/ppermute | solution.py:222
  10.1 13.9 %collective-permute-start.7 = (bf16[64,2176]{1,0:T(8,128)(2,1)S(1)}, bf16[64,2176]{1,0:T(8,128)(2,1)S(1)}, u32[]{:S(2)}, u32[]{:S(2)}) collective-permute-start(bf16[64,2176]{1,0:T(8,128)(2,1)S(1)} %get-tuple-element.26.refs_1_), channel_id=1, source_target_pairs={{4,0},{8,4},{12,8},{14,12},{10,14},{6,10},{2,6},{0,2},{5,1},{9,5},... | collective-permute-start | bytes 835592 | tf_op jit(solution)/shard_map/ppermute | solution.py:222
  10.5 13.5 %collective-permute-start.8 = (bf16[64,2176]{1,0:T(8,128)(2,1)S(1)}, bf16[64,2176]{1,0:T(8,128)(2,1)S(1)}, u32[]{:S(2)}, u32[]{:S(2)}) collective-permute-start(bf16[64,2176]{1,0:T(8,128)(2,1)S(1)} %get-tuple-element.25.refs_2_), channel_id=1, source_target_pairs={{4,0},{8,4},{12,8},{14,12},{10,14},{6,10},{2,6},{0,2},{5,1},{9,5},... | collective-permute-start | bytes 835592 | tf_op jit(solution)/shard_map/ppermute | solution.py:222
  24.0 11.9 %collective-permute-start.16 = (bf16[64,2176]{1,0:T(8,128)(2,1)S(1)}, bf16[64,2176]{1,0:T(8,128)(2,1)S(1)}, u32[]{:S(2)}, u32[]{:S(2)}) collective-permute-start(bf16[64,2176]{1,0:T(8,128)(2,1)S(1)} %collective-permute-done.7.refs_5_), channel_id=1, source_target_pairs={{4,0},{8,4},{12,8},{14,12},{10,14},{6,10},{2,6},{0,2},{5,1},{9,5},... | collective-permute-start | bytes 835592 | tf_op jit(solution)/shard_map/ppermute | solution.py:222
  24.0 12.1 %collective-permute-start.17 = (bf16[64,2176]{1,0:T(8,128)(2,1)S(1)}, bf16[64,2176]{1,0:T(8,128)(2,1)S(1)}, u32[]{:S(2)}, u32[]{:S(2)}) collective-permute-start(bf16[64,2176]{1,0:T(8,128)(2,1)S(1)} %collective-permute-done.8.refs_6_), channel_id=1, source_target_pairs={{4,0},{8,4},{12,8},{14,12},{10,14},{6,10},{2,6},{0,2},{5,1},{9,5},... | collective-permute-start | bytes 835592 | tf_op jit(solution)/shard_map/ppermute | solution.py:222
  52.2 30.8 %collective-permute-start.15 = (bf16[64,2176]{1,0:T(8,128)(2,1)S(1)}, bf16[64,2176]{1,0:T(8,128)(2,1)}, u32[]{:S(2)}, u32[]{:S(2)}) collective-permute-start(bf16[64,2176]{1,0:T(8,128)(2,1)S(1)} %collective-permute-done.13.refs_2_), channel_id=1, source_target_pairs={{0,1},{1,0},{2,3},{3,2},{4,5},{5,4},{6,7},{7,6},{8,9},{9,8},{10,11... | collective-permute-start | bytes 835592 | tf_op jit(solution)/shard_map/ppermute | solution.py:225
  52.9 30.7 %collective-permute-start.18 = (bf16[64,2176]{1,0:T(8,128)(2,1)S(1)}, bf16[64,2176]{1,0:T(8,128)(2,1)}, u32[]{:S(2)}, u32[]{:S(2)}) collective-permute-start(bf16[64,2176]{1,0:T(8,128)(2,1)S(1)} %collective-permute-done.16.refs_5_), channel_id=1, source_target_pairs={{0,1},{1,0},{2,3},{3,2},{4,5},{5,4},{6,7},{7,6},{8,9},{9,8},{10,11... | collective-permute-start | bytes 835592 | tf_op jit(solution)/shard_map/ppermute | solution.py:225
  54.1 29.5 %collective-permute-start.19 = (bf16[64,2176]{1,0:T(8,128)(2,1)S(1)}, bf16[64,2176]{1,0:T(8,128)(2,1)}, u32[]{:S(2)}, u32[]{:S(2)}) collective-permute-start(bf16[64,2176]{1,0:T(8,128)(2,1)S(1)} %collective-permute-done.17.refs_6_), channel_id=1, source_target_pairs={{0,1},{1,0},{2,3},{3,2},{4,5},{5,4},{6,7},{7,6},{8,9},{9,8},{10,11... | collective-permute-start | bytes 835592 | tf_op jit(solution)/shard_map/ppermute | solution.py:225
  57.2 26.9 %collective-permute-start.32 = (bf16[64,2176]{1,0:T(8,128)(2,1)}, bf16[64,2176]{1,0:T(8,128)(2,1)}, u32[]{:S(2)}, u32[]{:S(2)}) collective-permute-start(bf16[64,2176]{1,0:T(8,128)(2,1)} %collective-permute-done.30.refs_1_), channel_id=1, source_target_pairs={{0,1},{1,0},{2,3},{3,2},{4,5},{5,4},{6,7},{7,6},{8,9},{9,8},{10,11... | collective-permute-start | bytes 835592 | tf_op jit(solution)/shard_map/ppermute | solution.py:225
  59.2 25.0 %collective-permute-start.33 = (bf16[64,2176]{1,0:T(8,128)(2,1)}, bf16[64,2176]{1,0:T(8,128)(2,1)}, u32[]{:S(2)}, u32[]{:S(2)}) collective-permute-start(bf16[64,2176]{1,0:T(8,128)(2,1)} %collective-permute-done.31.refs_2_), channel_id=1, source_target_pairs={{0,1},{1,0},{2,3},{3,2},{4,5},{5,4},{6,7},{7,6},{8,9},{9,8},{10,11... | collective-permute-start | bytes 835592 | tf_op jit(solution)/shard_map/ppermute | solution.py:225
  83.0 22.1 %collective-permute-start.5 = (bf16[64,2176]{1,0:T(8,128)(2,1)S(1)}, bf16[64,2176]{1,0:T(8,128)(2,1)S(1)}, u32[]{:S(2)}, u32[]{:S(2)}) collective-permute-start(bf16[64,2176]{1,0:T(8,128)(2,1)S(1)} %collective-permute-done.3.refs_1_), channel_id=1, source_target_pairs={{0,1},{1,0},{2,3},{3,2},{4,5},{5,4},{6,7},{7,6},{8,9},{9,8},{10,11... | collective-permute-start | bytes 835592 | tf_op jit(solution)/shard_map/ppermute | solution.py:225
  83.6 21.7 %collective-permute-start.6 = (bf16[64,2176]{1,0:T(8,128)(2,1)S(1)}, bf16[64,2176]{1,0:T(8,128)(2,1)S(1)}, u32[]{:S(2)}, u32[]{:S(2)}) collective-permute-start(bf16[64,2176]{1,0:T(8,128)(2,1)S(1)} %collective-permute-done.4.refs_2_), channel_id=1, source_target_pairs={{0,1},{1,0},{2,3},{3,2},{4,5},{5,4},{6,7},{7,6},{8,9},{9,8},{10,11... | collective-permute-start | bytes 835592 | tf_op jit(solution)/shard_map/ppermute | solution.py:225
  83.7 22.0 %collective-permute-start.9 = (bf16[64,2176]{1,0:T(8,128)(2,1)S(1)}, bf16[64,2176]{1,0:T(8,128)(2,1)S(1)}, u32[]{:S(2)}, u32[]{:S(2)}) collective-permute-start(bf16[64,2176]{1,0:T(8,128)(2,1)S(1)} %collective-permute-done.7.refs_5_), channel_id=1, source_target_pairs={{0,1},{1,0},{2,3},{3,2},{4,5},{5,4},{6,7},{7,6},{8,9},{9,8},{10,11... | collective-permute-start | bytes 835592 | tf_op jit(solution)/shard_map/ppermute | solution.py:225
  84.1 21.6 %collective-permute-start.10 = (bf16[64,2176]{1,0:T(8,128)(2,1)S(1)}, bf16[64,2176]{1,0:T(8,128)(2,1)S(1)}, u32[]{:S(2)}, u32[]{:S(2)}) collective-permute-start(bf16[64,2176]{1,0:T(8,128)(2,1)S(1)} %collective-permute-done.8.refs_6_), channel_id=1, source_target_pairs={{0,1},{1,0},{2,3},{3,2},{4,5},{5,4},{6,7},{7,6},{8,9},{9,8},{10,11... | collective-permute-start | bytes 835592 | tf_op jit(solution)/shard_map/ppermute | solution.py:225
  84.2 37.3 %collective-permute-start.29 = (bf16[256,2048]{1,0:T(8,128)(2,1)S(1)}, bf16[256,2048]{1,0:T(8,128)(2,1)S(1)}, u32[]{:S(2)}, u32[]{:S(2)}) collective-permute-start(bf16[256,2048]{1,0:T(8,128)(2,1)S(1)} %get-tuple-element.22), channel_id=1, source_target_pairs={{0,1},{1,0},{2,3},{3,2},{4,5},{5,4},{6,7},{7,6},{8,9},{9,8},{10,11... | collective-permute-start | bytes 3145736 | tf_op jit(solution)/shard_map/ppermute | solution.py:225
  105.1 27.2 %collective-permute-start.20 = (bf16[256,2048]{1,0:T(8,128)(2,1)S(1)}, bf16[256,2048]{1,0:T(8,128)(2,1)S(1)}, u32[]{:S(2)}, u32[]{:S(2)}) collective-permute-start(bf16[256,2048]{1,0:T(8,128)(2,1)S(1)} %get-tuple-element.20), channel_id=1, source_target_pairs={{0,1},{1,0},{2,3},{3,2},{4,5},{5,4},{6,7},{7,6},{8,9},{9,8},{10,11... | collective-permute-start | bytes 3145736 | tf_op jit(solution)/shard_map/ppermute | solution.py:225
  105.3 12.0 %collective-permute-start.34 = (bf16[128,2048]{1,0:T(8,128)(2,1)S(1)}, bf16[128,2048]{1,0:T(8,128)(2,1)S(1)}, u32[]{:S(2)}, u32[]{:S(2)}) collective-permute-start(bf16[128,2048]{1,0:T(8,128)(2,1)S(1)} %get-tuple-element.24), channel_id=1, source_target_pairs={{0,1},{1,0},{2,3},{3,2},{4,5},{5,4},{6,7},{7,6},{8,9},{9,8},{10,11... | collective-permute-start | bytes 1572872 | tf_op jit(solution)/shard_map/ppermute | solution.py:225
  116.7 27.9 %collective-permute-start.11 = (bf16[256,2048]{1,0:T(8,128)(2,1)S(1)}, bf16[256,2048]{1,0:T(8,128)(2,1)S(1)}, u32[]{:S(2)}, u32[]{:S(2)}) collective-permute-start(bf16[256,2048]{1,0:T(8,128)(2,1)S(1)} %get-tuple-element.18), channel_id=1, source_target_pairs={{0,1},{1,0},{2,3},{3,2},{4,5},{5,4},{6,7},{7,6},{8,9},{9,8},{10,11... | collective-permute-start | bytes 3145736 | tf_op jit(solution)/shard_map/ppermute | solution.py:225
  122.0 18.0 %collective-permute-start.42 = (bf16[64,2048]{1,0:T(8,128)(2,1)S(1)}, bf16[64,2048]{1,0:T(8,128)(2,1)S(1)}, u32[]{:S(2)}, u32[]{:S(2)}) collective-permute-start(bf16[64,2048]{1,0:T(8,128)(2,1)S(1)} %shard_map.86), channel_id=1, source_target_pairs={{4,0},{8,4},{12,8},{14,12},{10,14},{6,10},{2,6},{0,2},{5,1},{9,5},... | collective-permute-start | bytes 786440 | tf_op jit(solution)/shard_map/ppermute | solution.py:222
  128.1 12.5 %collective-permute-start.39 = (bf16[64,2048]{1,0:T(8,128)(2,1)S(1)}, bf16[64,2048]{1,0:T(8,128)(2,1)S(1)}, u32[]{:S(2)}, u32[]{:S(2)}) collective-permute-start(bf16[64,2048]{1,0:T(8,128)(2,1)S(1)} %shard_map.82), channel_id=1, source_target_pairs={{0,4},{4,8},{8,12},{12,14},{14,10},{10,6},{6,2},{2,0},{1,5},{5,9},... | collective-permute-start | bytes 786440 | tf_op jit(solution)/shard_map/ppermute | solution.py:222
  140.7 18.4 %collective-permute-start.2 = (bf16[128,2048]{1,0:T(8,128)(2,1)S(1)}, bf16[128,2048]{1,0:T(8,128)(2,1)S(1)}, u32[]{:S(2)}, u32[]{:S(2)}) collective-permute-start(bf16[128,2048]{1,0:T(8,128)(2,1)S(1)} %get-tuple-element.16), channel_id=1, source_target_pairs={{0,1},{1,0},{2,3},{3,2},{4,5},{5,4},{6,7},{7,6},{8,9},{9,8},{10,11... | collective-permute-start | bytes 1572872 | tf_op jit(solution)/shard_map/ppermute | solution.py:225
  142.9 12.3 %collective-permute-start.47 = (bf16[64,2048]{1,0:T(8,128)(2,1)S(1)}, bf16[64,2048]{1,0:T(8,128)(2,1)S(1)}, u32[]{:S(2)}, u32[]{:S(2)}) collective-permute-start(bf16[64,2048]{1,0:T(8,128)(2,1)S(1)} %shard_map.91), channel_id=1, source_target_pairs={{0,4},{4,8},{8,12},{12,14},{14,10},{10,6},{6,2},{2,0},{1,5},{5,9},... | collective-permute-start | bytes 786440 | tf_op jit(solution)/shard_map/ppermute | solution.py:222
  144.6 13.8 %collective-permute-start.37 = (bf16[64,2048]{1,0:T(8,128)(2,1)S(1)}, bf16[64,2048]{1,0:T(8,128)(2,1)S(1)}, u32[]{:S(2)}, u32[]{:S(2)}) collective-permute-start(bf16[64,2048]{1,0:T(8,128)(2,1)S(1)} %shard_map.80), channel_id=1, source_target_pairs={{4,0},{8,4},{12,8},{14,12},{10,14},{6,10},{2,6},{0,2},{5,1},{9,5},... | collective-permute-start | bytes 786440 | tf_op jit(solution)/shard_map/ppermute | solution.py:222
  146.7 12.4 %collective-permute-start.44 = (bf16[64,2048]{1,0:T(8,128)(2,1)S(1)}, bf16[64,2048]{1,0:T(8,128)(2,1)S(1)}, u32[]{:S(2)}, u32[]{:S(2)}) collective-permute-start(bf16[64,2048]{1,0:T(8,128)(2,1)S(1)} %shard_map.88), channel_id=1, source_target_pairs={{4,0},{8,4},{12,8},{14,12},{10,14},{6,10},{2,6},{0,2},{5,1},{9,5},... | collective-permute-start | bytes 786440 | tf_op jit(solution)/shard_map/ppermute | solution.py:222
  (45 other events, 279.4 us)
